TPU v7x, 256 devices: a whole 4x4x8 slice. The times are simulated.
256 devices in a mesh: ep: 64 (over z, x, core), tp: 4 (over y).
Axes of the slice: x: 4, y: 4, z: 8, core: 2. Of those that a mesh axis runs over, the one named last changes fastest.
Arguments:
- queries: bfloat16 [32768, 2048], P('ep', 'tp'), may hold values from -6 to 6
- keys_values: bfloat16 [32768, 4, 128], P('ep', 'tp'), may hold values from -12 to 12
- sinks: float32 [32], P('tp'), may hold values from 1 to 5
- tokens_b: bfloat16 [32768, 2048], P(('ep', 'tp')), may hold values from -6 to 6
- norm_gain: float32 [2048], replicated, may hold values from 0.1 to 1.9
- routes: int32 [32768, 2], P(('ep', 'tp')), may hold values from 0 to 63, all different within a row; in each aligned block of 128 rows (0 to 127, 128 to 255, ...) at most 5 rows name the same one
- route_weights: float32 [32768, 2], P(('ep', 'tp')), may hold values from 0.1 to 0.9
- gate_weight: bfloat16 [64, 2048, 3584], P('ep', None, 'tp'), may hold values from -0.125 to 0.125
- up_weight: bfloat16 [64, 2048, 3584], P('ep', None, 'tp'), may hold values from -0.125 to 0.125
- down_weight: bfloat16 [64, 3584, 2048], P('ep', 'tp'), may hold values from -0.09375 to 0.09375
Outputs:
- attended: bfloat16 [32768, 2048], P('ep', 'tp')
- moe_out: bfloat16 [32768, 2048], P(('ep', 'tp'))
Inputs may be any that keep to these rules, and one draw needn't show every extreme that they name: `routes`: in each aligned block of 128 rows (the rows of one device) no expert is named by more than 5 rows; the 2 entries of a row differ.
All inputs are finite; a program needn't handle non-finite values.
Results may differ from a plain program's by a relative error of at most 0.012.
Values may be sent and summed in bfloat16 or wider, within the bound.
A program may use at most 128 MiB of HBM per device.

v0:
```python
import jax
import jax.numpy as jnp
from jax import lax
from jax.sharding import PartitionSpec as P

HEADS = 32
WINDOW = 128
NEG_SCORE = -1e30
EPSILON = 1e-06


def passed_along(value, axis, by):
    size = lax.axis_size(axis)
    pairs = [(i, i + by) for i in range(size) if 0 <= i + by < size]
    return lax.ppermute(value, axis, pairs)


def split_up(value, dim, size):
    before, after = (value.shape[:dim], value.shape[dim + 1 :])
    return jnp.moveaxis(value.reshape(*before, size, -1, *after), dim, 0)


def sent_and_summed(value, axis, dim):
    parts = split_up(value, dim, lax.axis_size(axis))
    arrived = lax.all_to_all(parts, axis, split_axis=0, concat_axis=0, tiled=True)
    return arrived.astype(jnp.float32).sum(axis=0)


def window_attention(queries, keys_values, sinks):
    row_count, kv_local, doubled = keys_values.shape
    head_size = doubled // 2
    heads_local = queries.shape[1] // head_size
    group_size = heads_local // kv_local
    window_rows = WINDOW
    block_count = row_count // window_rows
    earlier = passed_along(keys_values[row_count - window_rows :], "ep", 1)
    extended = jnp.concatenate([earlier, keys_values], axis=0)
    banded = jnp.concatenate(
        [
            extended[:row_count].reshape(block_count, window_rows, kv_local, doubled),
            extended[window_rows:].reshape(block_count, window_rows, kv_local, doubled),
        ],
        axis=1,
    )
    grouped = queries.reshape(block_count, window_rows, kv_local, group_size, head_size)
    scores = jnp.einsum(
        "nqkgd,nskd->nkgqs", grouped, banded[..., :head_size], preferred_element_type=jnp.float32
    ) * head_size ** (-0.5)
    first_head = lax.axis_index("tp") * heads_local
    head_ids = (first_head + jnp.arange(heads_local, dtype=jnp.int32)).astype(jnp.float32)
    slopes = (2.0 ** (-8.0 * (head_ids + 1.0) / HEADS)).reshape(1, kv_local, group_size, 1, 1)
    query_pos = jnp.arange(window_rows, dtype=jnp.int32)[:, None]
    key_pos = jnp.arange(2 * window_rows, dtype=jnp.int32)[None, :]
    distance = window_rows + query_pos - key_pos
    offset = lax.axis_index("ep") * row_count
    key_global = (
        offset + (jnp.arange(block_count, dtype=jnp.int32)[:, None] - 1) * window_rows + key_pos
    )
    allowed = (distance >= 0)[None] & (distance < window_rows)[None] & (key_global >= 0)[:, None, :]
    scores = jnp.where(
        allowed[:, None, None], scores - slopes * distance.astype(jnp.float32), NEG_SCORE
    )
    sink_logit = sinks.reshape(1, kv_local, group_size, 1, 1)
    peak_score = jnp.maximum(jnp.max(scores, axis=-1, keepdims=True), sink_logit)
    exponent = jnp.exp(scores - peak_score)
    denominator = jnp.sum(exponent, axis=-1, keepdims=True) + jnp.exp(sink_logit - peak_score)
    weights = (exponent / denominator).astype(jnp.bfloat16)
    mixed = jnp.einsum(
        "nkgqs,nskd->nqkgd", weights, banded[..., head_size:], preferred_element_type=jnp.float32
    )
    return mixed.astype(jnp.bfloat16).reshape(row_count, heads_local * head_size)


def slot_ranks(chosen, expert_count):
    onehot = (chosen[:, :, None] == jnp.arange(expert_count, dtype=jnp.int32)).astype(jnp.int32)
    return jnp.sum(jnp.cumsum(onehot, axis=1) * onehot, axis=2) - 1


def local(
    queries,
    keys_values,
    sinks,
    tokens_b,
    norm_gain,
    routes,
    route_weights,
    gate_weight,
    up_weight,
    down_weight,
):
    attended = window_attention(queries, keys_values, sinks)
    widened = tokens_b.astype(jnp.float32)
    scale = lax.rsqrt(jnp.mean(widened * widened, axis=-1, keepdims=True) + EPSILON)
    normed = (widened * scale * norm_gain).astype(jnp.bfloat16)
    own_rows, top_count = routes.shape
    model_width = normed.shape[1]
    expert_count = lax.axis_size("ep")
    capacity = max(2, 5 * own_rows * top_count // (4 * expert_count))
    pair_count = own_rows * top_count
    own_experts = routes.reshape(pair_count)
    gate_local = gate_weight[0]
    up_local = up_weight[0]
    own_slots = slot_ranks(own_experts[None], expert_count)[0]
    table = jnp.full((expert_count * capacity,), pair_count, jnp.int32)
    table = table.at[own_experts * capacity + own_slots].set(
        jnp.arange(pair_count, dtype=jnp.int32)
    )
    padded = jnp.concatenate([normed, jnp.zeros((1, model_width), jnp.bfloat16)], axis=0)
    outgoing = padded[table // top_count].reshape(expert_count, capacity, model_width)
    arrived = lax.all_to_all(outgoing, "ep", split_axis=0, concat_axis=0, tiled=True)
    piece = lax.all_gather(arrived, "tp", axis=0, tiled=True)
    flat_rows = piece.reshape(-1, model_width)
    gate_part = jnp.dot(flat_rows, gate_local, preferred_element_type=jnp.float32)
    up_part = jnp.dot(flat_rows, up_local, preferred_element_type=jnp.float32)
    result = (jax.nn.silu(gate_part) * up_part).astype(jnp.bfloat16)
    hidden = result.reshape(piece.shape[0], capacity, gate_local.shape[1]).reshape(
        -1, gate_local.shape[1]
    )
    down_local = down_weight[0]
    summed = sent_and_summed(
        jnp.dot(hidden, down_local, preferred_element_type=jnp.float32).astype(jnp.bfloat16),
        "tp",
        0,
    ).astype(jnp.bfloat16)
    returned = lax.all_to_all(
        summed.reshape(-1, capacity, model_width), "ep", split_axis=0, concat_axis=0, tiled=True
    )
    returned = returned.reshape(-1, model_width)
    picked = returned[own_experts * capacity + own_slots].astype(jnp.float32)
    weighted = picked.reshape(own_rows, top_count, model_width) * route_weights[:, :, None]
    moe_out = jnp.sum(weighted, axis=1).astype(jnp.bfloat16)
    return (attended, moe_out)


def solution(mesh):
    in_specs = (
        P("ep", "tp"),
        P("ep", "tp", None),
        P("tp"),
        P(("ep", "tp"), None),
        P(),
        P(("ep", "tp"), None),
        P(("ep", "tp"), None),
        P("ep", None, "tp"),
        P("ep", None, "tp"),
        P("ep", "tp", None),
    )
    out_specs = (P("ep", "tp"), P(("ep", "tp"), None))
    return jax.shard_map(local, mesh=mesh, in_specs=in_specs, out_specs=out_specs, check_vma=False)
```

profile of v0, /device:TPU:2, one launch (start us, length us, event | category | flops | bytes accessed | tf_op | source)
XLA Modules:
  0.0 333.7 jit_solution(17974118181820881681)
XLA Ops:
  14.4 2.4 gather_fusion
  17.4 63.1 %all_to_all.15 = bf16[64,5,2048]{2,1,0:T(8,128)(2,1)S(1)} all-to-all(bf16[64,5,2048]{2,1,0:T(8,128)(2,1)S(1)} %reshape.351), channel_id=1, replica_groups=mesh['ep'=64,'tp'=4] {'ep'}, dimensions={0} | all-to-all | bytes 2621440 | tf_op jit(solution)/shard_map/all_to_all | solution.py:110
  80.5 1.9 copy.39
  82.4 56.0 %all-gather.2.cloned.1.call-done = bf16[256,5,2048]{2,0,1:T(8,128)(2,1)} async-done(((bf16[64,5,2048]{2,0,1:T(8,128)(2,1)}), bf16[256,5,2048]{2,0,1:T(8,128)(2,1)}) %all-gather.2.cloned.1.call-update) | async-done | bytes 5242896 | tf_op jit(solution)/shard_map/all_gather | solution.py:111
  138.4 8.9 %copy.40 = bf16[256,5,2048]{2,1,0:T(8,128)(2,1)} copy(bf16[256,5,2048]{2,0,1:T(8,128)(2,1)} %all-gather.2.cloned.1.call-done) | data formatting | bytes 10485760 | tf_op jit(solution)/shard_map/all_gather | solution.py:111
  147.3 10.0 %reshape.352 = bf16[1280,2048]{1,0:T(8,128)(2,1)} reshape(bf16[256,5,2048]{2,1,0:T(8,128)(2,1)} %copy.40) | data formatting | bytes 10485760 | tf_op jit(solution)/shard_map/reshape | solution.py:112
  157.3 10.0 %fusion.4 = f32[1280,896]{1,0:T(8,128)} fusion(bf16[1280,2048]{1,0:T(8,128)(2,1)} %reshape.352, bf16[1,2048,896]{2,1,0:T(8,128)(2,1)} %param.17), kind=kOutput, calls=%fused_computation.12 | convolution fusion | flops 4697620480 | bytes 13500416 | tf_op jit(solution)/shard_map/dot_general | solution.py:113
  167.3 17.5 %convolution_convert_fusion = bf16[1280,2048]{1,0:T(8,128)(2,1)} fusion(bf16[1,896,2048]{2,1,0:T(8,128)(2,1)} %param.19, f32[1280,896]{1,0:T(8,128)} %fusion.4, bf16[1280,2048]{1,0:T(8,128)(2,1)} %reshape.352, bf16[1,2048,896]{2,1,0:T(8,128)(2,1)} %param.18), kind=kOutput, calls=%fused_computation.3 | convolution fusion | flops 9404743680 | bytes 22413312 | tf_op jit(solution)/shard_map/dot_general | solution.py:121
  184.8 5.2 %all-to-all-start.1 = ((bf16[4,320,2048]{2,1,0:T(8,128)(2,1)}), bf16[4,320,2048]{2,1,0:T(8,128)(2,1)}, u32[]{:S(2)}, u32[]{:S(2)}) async-start(bf16[4,320,2048]{2,1,0:T(8,128)(2,1)} %bitcast.85), calls=%async_computation.1 | async-start | bytes 10485760 | tf_op jit(solution)/shard_map/all_to_all | solution.py:25
  190.7 1.9 collective-permute-start
  193.0 57.3 %all-to-all-done.1 = bf16[4,320,2048]{2,1,0:T(8,128)(2,1)} async-done(((bf16[4,320,2048]{2,1,0:T(8,128)(2,1)}), bf16[4,320,2048]{2,1,0:T(8,128)(2,1)}, u32[]{:S(2)}, u32[]{:S(2)}) %all-to-all-start.1) | async-done | bytes 5242912 | tf_op jit(solution)/shard_map/all_to_all | solution.py:25
  250.2 3.6 %reduce_sum.51 = bf16[320,2048]{1,0:T(8,128)(2,1)S(1)} reduce(bf16[4,320,2048]{2,1,0:T(8,128)(2,1)} %all-to-all-done.1, bf16[]{:T(256)} %constant.73.clone.1), dimensions={0}, to_apply=%region_7.8 | reduce | flops 1966080 | bytes 6553602 | tf_op jit(solution)/shard_map/reduce_sum | solution.py:26
  253.9 1.6 reshape.354
  255.5 10.9 %all-to-all-start.2 = ((bf16[64,5,2048]{2,1,0:T(8,128)(2,1)}), bf16[64,5,2048]{2,1,0:T(8,128)(2,1)S(1)}, u32[]{:S(2)}, u32[]{:S(2)}) async-start(bf16[64,5,2048]{2,1,0:T(8,128)(2,1)} %reshape.354), calls=%async_computation.2 | async-start | bytes 4194304 | tf_op jit(solution)/shard_map/all_to_all | solution.py:125
  266.7 2.4 reshape.385
  269.8 1.4 pad_maximum_fusion.1
  272.3 2.3 fusion.6
  275.8 2.1 fusion.12
  277.9 1.6 copy.48
  279.5 1.4 reshape.386
  280.9 36.8 %all-to-all-done.2 = bf16[64,5,2048]{2,1,0:T(8,128)(2,1)S(1)} async-done(((bf16[64,5,2048]{2,1,0:T(8,128)(2,1)}), bf16[64,5,2048]{2,1,0:T(8,128)(2,1)S(1)}, u32[]{:S(2)}, u32[]{:S(2)}) %all-to-all-start.2) | async-done | bytes 1310752 | tf_op jit(solution)/shard_map/all_to_all | solution.py:125
  318.2 2.3 gather_fusion.1
  320.6 2.4 reshape.357
  323.0 3.9 %multiply_reduce_fusion = bf16[128,2048]{1,0:T(8,128)(2,1)} fusion(f32[128,2,2048]{2,1,0:T(2,128)S(1)} %reshape.357, f32[128,2]{1,0:T(8,128)S(1)} %copy-done.1), kind=kLoop, calls=%fused_computation.17 | loop fusion | flops 786432 | bytes 2622464 | tf_op jit(solution)/shard_map/reduce_sum | solution.py:131
  (54 shorter events, 12.5 us)
Async XLA Ops:
  7.2 131.3 %all-gather.2.cloned.1.call-start = ((), (), s32[]{:S(2)}) async-start(), calls=%async_computation.3 | async-start | bytes 6553600 | tf_op jit(solution)/shard_map/all_gather | solution.py:111
  184.8 5.2 %copy-start = (bf16[512,1,128]{2,0,1:T(8,128)(2,1)S(1)}, bf16[512,1,128]{2,0,1:T(8,128)(2,1)}, u32[]{:S(2)}) copy-start(bf16[512,1,128]{2,0,1:T(8,128)(2,1)} %param.11) | copy-start | bytes 393220
  184.8 65.4 %all-to-all-start.1 = ((bf16[4,320,2048]{2,1,0:T(8,128)(2,1)}), bf16[4,320,2048]{2,1,0:T(8,128)(2,1)}, u32[]{:S(2)}, u32[]{:S(2)}) async-start(bf16[4,320,2048]{2,1,0:T(8,128)(2,1)} %bitcast.85), calls=%async_computation.1 | async-start | bytes 10485760 | tf_op jit(solution)/shard_map/all_to_all | solution.py:25
  190.7 79.2 %collective-permute-start = (bf16[128,1,128]{2,0,1:T(8,128)(2,1)}, bf16[128,1,128]{2,0,1:T(8,128)(2,1)}, u32[]{:S(2)}, u32[]{:S(2)}) collective-permute-start(bf16[128,1,128]{2,0,1:T(8,128)(2,1)} %slice.18), channel_id=1, source_target_pairs={{0,4},{4,8},{8,12},{12,16},{16,20},{20,24},{24,28},{28,32},{32,36}... | collective-permute-start | bytes 98312 | tf_op jit(solution)/shard_map/ppermute | solution.py:15
  255.5 13.6 %copy-start.3 = (f32[128,2]{0,1:T(2,128)S(1)}, f32[128,2]{0,1:T(2,128)}, u32[]{:S(2)}) copy-start(f32[128,2]{0,1:T(2,128)} %param.16) | copy-start | bytes 3076
  255.5 62.1 %all-to-all-start.2 = ((bf16[64,5,2048]{2,1,0:T(8,128)(2,1)}), bf16[64,5,2048]{2,1,0:T(8,128)(2,1)S(1)}, u32[]{:S(2)}, u32[]{:S(2)}) async-start(bf16[64,5,2048]{2,1,0:T(8,128)(2,1)} %reshape.354), calls=%async_computation.2 | async-start | bytes 4194304 | tf_op jit(solution)/shard_map/all_to_all | solution.py:125
  266.7 7.9 %copy-start.2 = (f32[8]{0:T(128)S(1)}, f32[8]{0:T(128)}, u32[]{:S(2)}) copy-start(f32[8]{0:T(128)} %param.12) | copy-start | bytes 100
  318.2 4.7 %copy-start.1 = (f32[128,2]{1,0:T(8,128)S(1)}, f32[128,2]{1,0:T(8,128)}, u32[]{:S(2)}) copy-start(f32[128,2]{1,0:T(8,128)} %copy.41) | copy-start | bytes 3076
Sparse Core Ops, SparseCore 0:
  82.5 55.8 all-gather.1
where the time goes:
time: 335 us; the launch traced here: 334 us
  waiting for transfers between devices  150 us (45%)
  blocking collectives  63.1 us (19%)
  local copies, waits for them, and re-layouts  41.7 us (12%)
  matrix products  31.8 us (9%)
  starting transfers between devices  18 us (5%)
  other arithmetic  14.7 us (4%)
  between operations  14.3 us (4%)
    all_to_all x1, blocking collectives, local(): lax.all_to_all(outgoing, 'ep', split_axis=0, concat_axis=0, tiled=True)  63.1 us
    all_to_all x1, waiting for transfers between devices, sent_and_summed(): lax.all_to_all(parts, axis, split_axis=0, concat_axis=0, tiled=True)  57.3 us
    all_gather x1, waiting for transfers between devices, local(): piece = lax.all_gather(arrived, 'tp', axis=0, tiled=True)  56 us
    all_to_all x1, waiting for transfers between devices, local(): lax.all_to_all(summed.reshape(-1, capacity, model_width), 'ep', split_axi...  36.8 us
    dot_general x1, matrix products, local(): jnp.dot(hidden, down_local, preferred_element_type=jnp.float32)  17.5 us
    all_to_all x1, starting transfers between devices, local(): lax.all_to_all(summed.reshape(-1, capacity, model_width), 'ep', split_axi...  10.9 us
    reshape x1, local copies, waits for them, and re-layouts, local(): flat_rows = piece.reshape(-1, model_width)  10 us
    dot_general x1, matrix products, local(): jnp.dot(flat_rows, gate_local, preferred_element_type=jnp.float32)  9.96 us
  transfers between devices with their start and end apart: 4, of which 3 were waited for; matrix products, arithmetic and copies ran while one was open for 6% of the time, Pallas kernels for 0%

commit v1 on v0

--- a/solution.py
+++ b/solution.py
@@ -108,7 +108,9 @@
     padded = jnp.concatenate([normed, jnp.zeros((1, model_width), jnp.bfloat16)], axis=0)
     outgoing = padded[table // top_count].reshape(expert_count, capacity, model_width)
     arrived = lax.all_to_all(outgoing, "ep", split_axis=0, concat_axis=0, tiled=True)
-    piece = lax.all_gather(arrived, "tp", axis=0, tiled=True)
+    piece = jnp.concatenate(
+        lax.all_to_all(jnp.stack([arrived] * lax.axis_size("tp")), "tp", 0, 0), axis=0
+    )
     flat_rows = piece.reshape(-1, model_width)
     gate_part = jnp.dot(flat_rows, gate_local, preferred_element_type=jnp.float32)
     up_part = jnp.dot(flat_rows, up_local, preferred_element_type=jnp.float32)

time: 335 us -> 322 us (0.961)
  blocking collectives: 63.1 us -> 126 us
  waiting for transfers between devices: 150 us -> 91.5 us
  between operations: 14.3 us -> 0.93 us
    all_to_all x0 -> x1, blocking collectives: none -> 62.8 us  [local(): lax.all_to_all(jnp.stack([arrived] * lax.axis_size('tp')), 'tp', 0, 0)]
    all_gather x1 -> x0, waiting for transfers between devices: 56 us -> none  [local(): piece = lax.all_gather(arrived, 'tp', axis=0, tiled=True)]
    another operation x6 -> x8, local copies, waits for them, and re-layouts: 2.67 us -> 13.4 us  [the longest x1 10 us: local(): flat_rows = piece.reshape(-1, model_width)]
    reshape x1 -> x0, local copies, waits for them, and re-layouts: 10 us -> none  [local(): flat_rows = piece.reshape(-1, model_width)]
    all_gather x1 -> x0, local copies, waits for them, and re-layouts: 8.89 us -> none  [local(): piece = lax.all_gather(arrived, 'tp', axis=0, tiled=True)]
    all_to_all x0 -> x1, local copies, waits for them, and re-layouts: none -> 6.78 us  [local(): lax.all_to_all(jnp.stack([arrived] * lax.axis_size('tp')), 'tp', 0, 0)]
  transfers between devices with their start and end apart: 4 -> 3, of which waited for: 3 -> 2; matrix products, arithmetic and copies ran while one was open for 6% -> 6% of each run, Pallas kernels for 0% -> 0%
where the time goes in v1:
time: 322 us; the launch traced here: 321 us
  blocking collectives  126 us (39%)
  waiting for transfers between devices  91.5 us (28%)
  local copies, waits for them, and re-layouts  39.2 us (12%)
  matrix products  31.8 us (10%)
  starting transfers between devices  16.5 us (5%)
  other arithmetic  14.7 us (5%)
    all_to_all x1, blocking collectives, local(): lax.all_to_all(outgoing, 'ep', split_axis=0, concat_axis=0, tiled=True)  63.1 us
    all_to_all x1, blocking collectives, local(): lax.all_to_all(jnp.stack([arrived] * lax.axis_size('tp')), 'tp', 0, 0)  62.8 us
    all_to_all x1, waiting for transfers between devices, sent_and_summed(): lax.all_to_all(parts, axis, split_axis=0, concat_axis=0, tiled=True)  54.8 us
    all_to_all x1, waiting for transfers between devices, local(): lax.all_to_all(summed.reshape(-1, capacity, model_width), 'ep', split_axi...  36.8 us
    dot_general x1, matrix products, local(): jnp.dot(hidden, down_local, preferred_element_type=jnp.float32)  17.5 us
    another operation x1, local copies, waits for them, and re-layouts, local(): flat_rows = piece.reshape(-1, model_width)  10 us
    dot_general x1, matrix products, local(): jnp.dot(flat_rows, gate_local, preferred_element_type=jnp.float32)  9.96 us
    all_to_all x1, starting transfers between devices, local(): lax.all_to_all(summed.reshape(-1, capacity, model_width), 'ep', split_axi...  9.4 us
  transfers between devices with their start and end apart: 3, of which 2 were waited for; matrix products, arithmetic and copies ran while one was open for 6% of the time, Pallas kernels for 0%

profile of v1, /device:TPU:2, one launch (start us, length us, event | category | flops | bytes accessed | tf_op | source)
XLA Modules:
  0.0 320.6 jit_solution(3518673461778295815)
XLA Ops:
  3.9 1.4 scatter_custom_fusion
  7.8 2.4 gather_fusion
  10.8 63.1 %all_to_all.20 = bf16[64,5,2048]{2,1,0:T(8,128)(2,1)S(1)} all-to-all(bf16[64,5,2048]{2,1,0:T(8,128)(2,1)S(1)} %reshape.350), channel_id=1, replica_groups=mesh['ep'=64,'tp'=4] {'ep'}, dimensions={0} | all-to-all | bytes 2621440 | tf_op jit(solution)/shard_map/all_to_all | solution.py:110
  75.4 62.8 %all_to_all.21 = bf16[4,64,5,2048]{3,1,2,0:T(8,128)(2,1)S(1)} all-to-all(bf16[4,64,5,2048]{3,1,2,0:T(8,128)(2,1)S(1)} %stack.2), channel_id=1, replica_groups=mesh['ep'=64,'tp'=4] {'tp'}, dimensions={0} | all-to-all | bytes 10485760 | tf_op jit(solution)/shard_map/all_to_all | solution.py:112
  138.2 6.8 %copy.40 = bf16[4,64,5,2048]{3,2,1,0:T(8,128)(2,1)} copy(bf16[4,64,5,2048]{3,1,2,0:T(8,128)(2,1)S(1)} %all_to_all.21) | data formatting | bytes 10485760 | tf_op jit(solution)/shard_map/all_to_all | solution.py:112
  145.0 10.0 %reshape_reshape.3 = bf16[1280,2048]{1,0:T(8,128)(2,1)} reshape(bf16[4,64,5,2048]{3,2,1,0:T(8,128)(2,1)} %copy.40) | data formatting | bytes 10485760 | tf_op jit(solution)/shard_map/reshape;reshape | solution.py:114
  155.0 10.0 %fusion.4 = f32[1280,896]{1,0:T(8,128)} fusion(bf16[1280,2048]{1,0:T(8,128)(2,1)} %reshape_reshape.3, bf16[1,2048,896]{2,1,0:T(8,128)(2,1)} %param.17), kind=kOutput, calls=%fused_computation.12 | convolution fusion | flops 4697620480 | bytes 13500416 | tf_op jit(solution)/shard_map/dot_general | solution.py:115
  165.0 17.5 %convolution_convert_fusion = bf16[1280,2048]{1,0:T(8,128)(2,1)} fusion(bf16[1,896,2048]{2,1,0:T(8,128)(2,1)} %param.19, f32[1280,896]{1,0:T(8,128)} %fusion.4, bf16[1280,2048]{1,0:T(8,128)(2,1)} %reshape_reshape.3, bf16[1,2048,896]{2,1,0:T(8,128)(2,1)} %param.18), kind=kOutput, calls=%fused_computation.3 | convolution fusion | flops 9404743680 | bytes 22413312 | tf_op jit(solution)/shard_map/dot_general | solution.py:123
  182.5 5.2 %all-to-all-start.2 = ((bf16[4,320,2048]{2,1,0:T(8,128)(2,1)}), bf16[4,320,2048]{2,1,0:T(8,128)(2,1)}, u32[]{:S(2)}, u32[]{:S(2)}) async-start(bf16[4,320,2048]{2,1,0:T(8,128)(2,1)} %bitcast.85), calls=%async_computation.2 | async-start | bytes 10485760 | tf_op jit(solution)/shard_map/all_to_all | solution.py:25
  188.3 1.9 collective-permute-start
  190.6 54.8 %all-to-all-done.2 = bf16[4,320,2048]{2,1,0:T(8,128)(2,1)} async-done(((bf16[4,320,2048]{2,1,0:T(8,128)(2,1)}), bf16[4,320,2048]{2,1,0:T(8,128)(2,1)}, u32[]{:S(2)}, u32[]{:S(2)}) %all-to-all-start.2) | async-done | bytes 5242912 | tf_op jit(solution)/shard_map/all_to_all | solution.py:25
  245.4 3.6 %reduce_sum.51 = bf16[320,2048]{1,0:T(8,128)(2,1)S(1)} reduce(bf16[4,320,2048]{2,1,0:T(8,128)(2,1)} %all-to-all-done.2, bf16[]{:T(256)} %constant.73.clone.1), dimensions={0}, to_apply=%region_7.8 | reduce | flops 1966080 | bytes 6553602 | tf_op jit(solution)/shard_map/reduce_sum | solution.py:26
  249.0 1.6 reshape.352
  250.7 9.4 %all-to-all-start.3 = ((bf16[64,5,2048]{2,1,0:T(8,128)(2,1)}), bf16[64,5,2048]{2,1,0:T(8,128)(2,1)S(1)}, u32[]{:S(2)}, u32[]{:S(2)}) async-start(bf16[64,5,2048]{2,1,0:T(8,128)(2,1)} %reshape.352), calls=%async_computation.3 | async-start | bytes 4194304 | tf_op jit(solution)/shard_map/all_to_all | solution.py:127
  260.4 2.4 reshape.383
  263.5 1.4 pad_maximum_fusion.1
  266.0 2.3 fusion.6
  269.5 2.1 fusion.12
  271.6 1.6 copy.48
  273.2 1.4 reshape.384
  274.6 36.8 %all-to-all-done.3 = bf16[64,5,2048]{2,1,0:T(8,128)(2,1)S(1)} async-done(((bf16[64,5,2048]{2,1,0:T(8,128)(2,1)}), bf16[64,5,2048]{2,1,0:T(8,128)(2,1)S(1)}, u32[]{:S(2)}, u32[]{:S(2)}) %all-to-all-start.3) | async-done | bytes 1310752 | tf_op jit(solution)/shard_map/all_to_all | solution.py:127
  311.9 2.3 gather_fusion.1
  314.3 2.4 reshape.355
  316.6 3.9 %multiply_reduce_fusion = bf16[128,2048]{1,0:T(8,128)(2,1)} fusion(f32[128,2,2048]{2,1,0:T(2,128)S(1)} %reshape.355, f32[128,2]{1,0:T(8,128)S(1)} %copy-done.1), kind=kLoop, calls=%fused_computation.17 | loop fusion | flops 786432 | bytes 2622464 | tf_op jit(solution)/shard_map/reduce_sum | solution.py:133
  (53 shorter events, 12.6 us)
Async XLA Ops:
  182.5 5.2 %copy-start = (bf16[512,1,128]{2,0,1:T(8,128)(2,1)S(1)}, bf16[512,1,128]{2,0,1:T(8,128)(2,1)}, u32[]{:S(2)}) copy-start(bf16[512,1,128]{2,0,1:T(8,128)(2,1)} %param.11) | copy-start | bytes 393220
  182.5 62.9 %all-to-all-start.2 = ((bf16[4,320,2048]{2,1,0:T(8,128)(2,1)}), bf16[4,320,2048]{2,1,0:T(8,128)(2,1)}, u32[]{:S(2)}, u32[]{:S(2)}) async-start(bf16[4,320,2048]{2,1,0:T(8,128)(2,1)} %bitcast.85), calls=%async_computation.2 | async-start | bytes 10485760 | tf_op jit(solution)/shard_map/all_to_all | solution.py:25
  188.3 75.2 %collective-permute-start = (bf16[128,1,128]{2,0,1:T(8,128)(2,1)}, bf16[128,1,128]{2,0,1:T(8,128)(2,1)}, u32[]{:S(2)}, u32[]{:S(2)}) collective-permute-start(bf16[128,1,128]{2,0,1:T(8,128)(2,1)} %slice.18), channel_id=1, source_target_pairs={{0,4},{4,8},{8,12},{12,16},{16,20},{20,24},{24,28},{28,32},{32,36}... | collective-permute-start | bytes 98312 | tf_op jit(solution)/shard_map/ppermute | solution.py:15
  250.7 12.1 %copy-start.3 = (f32[128,2]{0,1:T(2,128)S(1)}, f32[128,2]{0,1:T(2,128)}, u32[]{:S(2)}) copy-start(f32[128,2]{0,1:T(2,128)} %param.16) | copy-start | bytes 3076
  250.7 60.6 %all-to-all-start.3 = ((bf16[64,5,2048]{2,1,0:T(8,128)(2,1)}), bf16[64,5,2048]{2,1,0:T(8,128)(2,1)S(1)}, u32[]{:S(2)}, u32[]{:S(2)}) async-start(bf16[64,5,2048]{2,1,0:T(8,128)(2,1)} %reshape.352), calls=%async_computation.3 | async-start | bytes 4194304 | tf_op jit(solution)/shard_map/all_to_all | solution.py:127
  260.4 7.9 %copy-start.2 = (f32[8]{0:T(128)S(1)}, f32[8]{0:T(128)}, u32[]{:S(2)}) copy-start(f32[8]{0:T(128)} %param.12) | copy-start | bytes 100
  311.9 4.7 %copy-start.1 = (f32[128,2]{1,0:T(8,128)S(1)}, f32[128,2]{1,0:T(8,128)}, u32[]{:S(2)}) copy-start(f32[128,2]{1,0:T(8,128)} %copy.41) | copy-start | bytes 3076
